TPU v7x, 32 devices: a whole 2x2x4 slice. The times are simulated.
32 devices in a mesh: sp: 8 (over z, core), tp: 4 (over y, x).
Axes of the slice: x: 2, y: 2, z: 4, core: 2. Of those that a mesh axis runs over, the one named last changes fastest.
Arguments:
- query_a: bfloat16 [1024, 1024], P('tp', 'sp'), may hold values from -16 to 16
- key_a: bfloat16 [1024, 1024], P('tp', 'sp'), may hold values from -6 to 6
- value_a: bfloat16 [1024, 1024], P('tp', 'sp'), may hold values from -6 to 6
- cumlog_a: float32 [16, 1024], P('tp'), as said below
- query_b: bfloat16 [2048, 1024], P('tp', 'sp'), may hold values from -16 to 16
- key_b: bfloat16 [2048, 1024], P('tp', 'sp'), may hold values from -6 to 6
- value_b: bfloat16 [2048, 1024], P('tp', 'sp'), may hold values from -6 to 6
- cumlog_b: float32 [16, 1024], P('tp'), as said below
- out_weight_a: bfloat16 [1024, 2048], P('tp'), may hold values from -0.375 to 0.375
- out_weight_b: bfloat16 [2048, 2048], P('tp'), may hold values from -0.25 to 0.25
- residual: bfloat16 [1024, 2048], P(('sp', 'tp')), may hold values from -6 to 6
- norm_gain: float32 [2048], replicated, may hold values from 0.1 to 1.9
- expert_ids: int32 [1024, 2], P('sp'), may hold values from 0 to 7, as said below
- route_weight: float32 [1024, 2], P('sp'), may hold values from 0.1 to 1
- gate_w: bfloat16 [8, 2048, 1024], P('sp', None, 'tp'), may hold values from -0.125 to 0.125
- up_w: bfloat16 [8, 2048, 1024], P('sp', None, 'tp'), may hold values from -0.125 to 0.125
- down_w: bfloat16 [8, 1024, 2048], P('sp', None, 'tp'), may hold values from -0.1875 to 0.1875
Outputs:
- layer_out: bfloat16 [1024, 2048], P('sp', 'tp')
Inputs may be any that keep to these rules, and one draw needn't show every extreme that they name: `expert_ids`: each row names two different experts of one group (expert e is in group e // 2). In every aligned block of 128 rows (one index of sp) no expert is named more than 64 times, and every expert of one group, the same group for all blocks, is named exactly 64 times. `cumlog_a`: along positions the values of each head never increase. `cumlog_b`: along positions the values of each head never increase.
All inputs are finite; a program needn't handle non-finite values.
Results may differ from a plain program's by a relative error of at most 0.017.
Values may be sent and summed in bfloat16 or wider, within the bound.
A program may use at most 64 MiB of HBM per device.

v0:
```python
import jax
import jax.numpy as jnp
from jax import lax
from jax.sharding import PartitionSpec as P

HDA = 64
HDB = 128
GROUPS = 4
TOP = 2


norm_eps = 1e-05


def fold_group(state, queries, keys_piece, values_piece, cum_query, cum_key, visible, head_size):
    best, total, accum = state
    heads = best.shape[0]
    count = keys_piece.shape[1]
    key_grid = keys_piece.reshape(heads, head_size, count)
    value_grid = values_piece.reshape(heads, head_size, count)
    scores = jnp.einsum(
        "hdq,hdk->hqk", queries, key_grid, preferred_element_type=jnp.float32
    ) * head_size ** (-0.5)
    scores = scores + cum_query[:, :, None] - cum_key[:, None, :]
    scores = jnp.where(visible, scores, -jnp.inf)
    best_new = jnp.max(scores, axis=-1)
    shift = jnp.where(best_new > -jnp.inf, best_new, 0.0)
    keep_old = jnp.exp(best - shift)
    weights = jnp.exp(scores - shift[:, :, None])
    total_new = total * keep_old + jnp.sum(weights, axis=-1)
    added = jnp.einsum(
        "hqk,hdk->hdq", weights.astype(jnp.bfloat16), value_grid, preferred_element_type=jnp.float32
    )
    return (best_new, total_new, accum * keep_old[:, None, :] + added)


def empty_state(heads, head_size, length):
    return (
        jnp.full((heads, length), -jnp.inf, jnp.float32),
        jnp.zeros((heads, length), jnp.float32),
        jnp.zeros((heads, head_size, length), jnp.float32),
    )


def finish_state(state):
    accum = state[2] / state[1][:, None, :]
    return accum.astype(jnp.bfloat16).reshape(-1, accum.shape[2])


def per_device(
    query_a,
    key_a,
    value_a,
    cumlog_a,
    query_b,
    key_b,
    value_b,
    cumlog_b,
    out_weight_a,
    out_weight_b,
    residual,
    norm_gain,
    expert_ids,
    route_weight,
    gate_w,
    up_w,
    down_w,
):
    local_tokens = query_a.shape[1]
    heads_a = cumlog_a.shape[0]
    heads_b = cumlog_b.shape[0]
    my_start = lax.axis_index("sp") * local_tokens
    last_query = my_start + local_tokens - 1
    query_pos = my_start + jnp.arange(local_tokens, dtype=jnp.int32)
    cum_query_a = lax.dynamic_slice_in_dim(cumlog_a, my_start, local_tokens, 1)
    cum_query_b = lax.dynamic_slice_in_dim(cumlog_b, my_start, local_tokens, 1)
    grid_a = query_a.reshape(heads_a, HDA, local_tokens)
    grid_b = query_b.reshape(heads_b, HDB, local_tokens)
    keys_a = lax.all_gather(key_a, "sp", axis=1, tiled=True)
    vals_a = lax.all_gather(value_a, "sp", axis=1, tiled=True)
    keys_b = lax.all_gather(key_b, "sp", axis=1, tiled=True)
    vals_b = lax.all_gather(value_b, "sp", axis=1, tiled=True)
    count = keys_a.shape[1]

    def visit(state):
        key_pos = jnp.arange(count, dtype=jnp.int32)
        visible = key_pos[None, None, :] <= query_pos[None, :, None]
        new_a = fold_group(state[0], grid_a, keys_a, vals_a, cum_query_a, cumlog_a, visible, HDA)
        new_b = fold_group(state[1], grid_b, keys_b, vals_b, cum_query_b, cumlog_b, visible, HDB)
        return (new_a, new_b)

    def leave(state):
        return state

    state_a, state_b = lax.cond(
        jnp.int32(0) <= last_query,
        visit,
        leave,
        (empty_state(heads_a, HDA, local_tokens), empty_state(heads_b, HDB, local_tokens)),
    )
    attn_a = finish_state(state_a)
    attn_b = finish_state(state_b)
    term = lax.dot_general(
        attn_a, out_weight_a, (((0,), (0,)), ((), ())), preferred_element_type=jnp.float32
    )
    mixed = lax.psum_scatter(
        (
            term
            + lax.dot_general(
                attn_b, out_weight_b, (((0,), (0,)), ((), ())), preferred_element_type=jnp.float32
            )
        ).astype(jnp.bfloat16),
        "tp",
        scatter_dimension=0,
        tiled=True,
    ).astype(jnp.float32)
    summed = residual.astype(jnp.float32) + mixed
    center = summed - jnp.mean(summed, axis=-1, keepdims=True)
    variance = jnp.mean(center * center, axis=-1, keepdims=True)
    normed = (center * lax.rsqrt(variance + norm_eps) * norm_gain).astype(jnp.bfloat16)
    normed_all = lax.all_gather(normed, "tp", axis=0, tiled=True)
    experts = lax.axis_size("sp")
    group_size = experts // GROUPS
    capacity = local_tokens // group_size
    features = normed_all.shape[1]
    flat_ids = expert_ids.reshape(-1)
    marks = (flat_ids[:, None] == jnp.arange(experts, dtype=jnp.int32)[None, :]).astype(jnp.int32)
    rank = jnp.sum((jnp.cumsum(marks, axis=0) - marks) * marks, axis=1)
    slot = flat_ids * capacity + rank
    token_of = jnp.arange(local_tokens * TOP, dtype=jnp.int32) // TOP
    table = jnp.zeros((experts * capacity,), jnp.int32).at[slot].set(token_of)
    filled = jnp.zeros((experts * capacity,), jnp.bfloat16).at[slot].set(1.0)
    send = (normed_all[table] * filled[:, None]).reshape(experts, capacity, features)
    rows = lax.all_to_all(send, "sp", split_axis=0, concat_axis=0, tiled=True)
    sources, items, row_width = rows.shape
    flat_rows = rows.reshape(sources * items, row_width)
    gate = jnp.dot(flat_rows, gate_w[0], preferred_element_type=jnp.float32)
    upper = jnp.dot(flat_rows, up_w[0], preferred_element_type=jnp.float32)
    hidden = (jax.nn.silu(gate) * upper).astype(jnp.bfloat16).reshape(sources, items, -1)
    hidden_all = lax.all_gather(hidden, "tp", axis=2, tiled=True)
    result = jnp.dot(
        hidden_all.reshape(sources * items, -1), down_w[0], preferred_element_type=jnp.float32
    )
    result = result.astype(jnp.bfloat16).reshape(sources, items, -1)
    returned = lax.all_to_all(result, "sp", split_axis=0, concat_axis=0, tiled=True)
    flat_back = returned.reshape(experts * capacity, -1)
    picked = flat_back[slot].reshape(local_tokens, TOP, -1).astype(jnp.float32)
    routed = jnp.sum(picked * route_weight[:, :, None], axis=1)
    columns = routed.shape[1]
    own_cols = lax.dynamic_slice_in_dim(normed_all, lax.axis_index("tp") * columns, columns, 1)
    return (own_cols.astype(jnp.float32) + routed).astype(jnp.bfloat16)


def solution(mesh):
    placed = (
        P("tp", "sp"),
        P("tp", "sp"),
        P("tp", "sp"),
        P("tp", None),
        P("tp", "sp"),
        P("tp", "sp"),
        P("tp", "sp"),
        P("tp", None),
        P("tp", None),
        P("tp", None),
        P(("sp", "tp"), None),
        P(),
        P("sp", None),
        P("sp", None),
        P("sp", None, "tp"),
        P("sp", None, "tp"),
        P("sp", None, "tp"),
    )
    return jax.shard_map(
        per_device, mesh=mesh, in_specs=placed, out_specs=P("sp", "tp"), check_vma=False
    )
```

profile of v0, /device:TPU:0, one launch (start us, length us, event | category | flops | bytes accessed | tf_op | source)
XLA Modules:
  0.0 229.1 jit_solution(7319173430591822474)
XLA Ops:
  6.5 0.7 all-gather.4.cloned.1.call-update
  7.3 0.7 all-gather.6.cloned.1.call-update
  8.1 0.8 copy.27
  8.8 0.1 eq.29
  9.0 0.7 eq.25
  9.7 0.7 broadcast_multiply_fusion.1
  10.4 0.1 copy.26
  10.5 0.1 mul.103
  10.6 17.6 %all_gather.18 = bf16[256,1024]{1,0:T(8,128)(2,1)S(1)} all-gather(bf16[256,128]{1,0:T(8,128)(2,1)} %param.20), channel_id=1, replica_groups=mesh['sp'=8,'tp'=4] {'sp'}, dimensions={1}, use_global_device_ids=true | all-gather | bytes 589824 | tf_op jit(solution)/shard_map/all_gather | solution.py:79
  28.2 14.7 %all_gather.19 = bf16[256,1024]{1,0:T(8,128)(2,1)S(1)} all-gather(bf16[256,128]{1,0:T(8,128)(2,1)} %param.21), channel_id=1, replica_groups=mesh['sp'=8,'tp'=4] {'sp'}, dimensions={1}, use_global_device_ids=true | all-gather | bytes 589824 | tf_op jit(solution)/shard_map/all_gather | solution.py:80
  42.9 19.9 %all-gather.6.cloned.1.call-done = bf16[512,1024]{1,0:T(8,128)(2,1)} async-done(((bf16[512,128]{1,0:T(8,128)(2,1)}), bf16[512,1024]{1,0:T(8,128)(2,1)}) %all-gather.6.cloned.1.call-update) | async-done | bytes 1048592 | tf_op jit(solution)/shard_map/all_gather | solution.py:82
  62.8 7.6 %conditional.1 = (f32[4,128]{1,0:T(4,128)S(1)}, f32[4,64,128]{2,1,0:T(8,128)S(1)}, f32[4,128]{1,0:T(4,128)S(1)}, f32[4,128,128]{2,1,0:T(8,128)S(1)}) conditional(s32[]{:T(128)} %convert_element_type.59, () %tuple.20, (s32[]{:T(128)}, s32[128]{0:T(128)S(1)}, bf16[256,128]{1,0:T(8,128)(2,1)}, bf16[256,1024]{1,0:T(8,128)(2,1)S(1)}, f32[4,1024]{1,0:T(4,128)}, ...), branch_computations={%region_0.0_spmd, %region_1.6_spmd} | conditional | flops 412324992 | bytes 26306234 | solution.py:95
  62.8 0.8 constant_dynamic-slice_fusion
  63.6 0.1 iota_compare_fusion
  63.7 1.6 fusion.27
  65.4 0.5 fusion.1
  65.9 0.6 fusion.5
  66.6 0.8 fusion.28
  67.4 0.5 fusion.3
  68.0 1.3 fusion.4
  69.3 1.1 copy.32
  70.4 1.6 fusion.29
  72.1 1.3 fusion.12
  73.4 0.6 reduce-window.6
  74.0 0.2 slice_reduce_fusion
  74.3 0.1 fusion.21
  74.4 1.4 scatter_custom_fusion
  75.8 2.2 scatter_custom_fusion.1
  78.0 19.3 %reduce-scatter.2.cloned.1.call-done = bf16[32,2048]{1,0:T(8,128)(2,1)} async-done(((bf16[128,2048]{1,0:T(8,128)(2,1)}), bf16[32,2048]{1,0:T(8,128)(2,1)}) %reduce-scatter.2.cloned.1.call-update) | async-done | bytes 131088 | tf_op jit(solution)/shard_map/reduce_scatter | solution.py:106
  97.3 1.0 fusion.19
  98.4 1.1 multiply_reduce_fusion.1
  99.5 1.0 multiply_convert_fusion
  100.5 10.2 %all_gather.22 = bf16[128,2048]{1,0:T(8,128)(2,1)S(1)} all-gather(bf16[32,2048]{1,0:T(8,128)(2,1)S(1)} %multiply_convert_fusion), channel_id=1, replica_groups=mesh['sp'=8,'tp'=4] {'tp'}, dimensions={0}, use_global_device_ids=true | all-gather | bytes 655360 | tf_op jit(solution)/shard_map/all_gather | solution.py:121
  110.8 3.3 %gather_fusion = bf16[512,2048]{1,0:T(8,128)(2,1)} fusion(bf16[128,2048]{1,0:T(8,128)(2,1)S(1)} %all_gather.22, s32[1024]{0:T(1024)S(1)} %pad_clamp_fusion.1), kind=kCustom, calls=%fused_computation | custom fusion | bytes 4196352 | tf_op jit(solution)/shard_map/gather | solution.py:133
  114.1 1.8 broadcast_multiply_fusion
  115.9 53.6 %all_to_all.10 = bf16[8,64,2048]{2,1,0:T(8,128)(2,1)S(1)} all-to-all(bf16[8,64,2048]{2,1,0:T(8,128)(2,1)S(1)} %broadcast_multiply_fusion), channel_id=1, replica_groups=mesh['sp'=8,'tp'=4] {'sp'}, dimensions={0} | all-to-all | bytes 4194304 | tf_op jit(solution)/shard_map/all_to_all | solution.py:134
  169.5 0.7 fusion.16
  170.3 0.5 copy-done.8
  170.8 1.4 fusion.13
  172.2 24.5 %all-gather.8.cloned.1.call-done = bf16[8,64,1024]{2,1,0:T(8,128)(2,1)} async-done(((bf16[8,64,256]{2,1,0:T(8,128)(2,1)}), bf16[8,64,1024]{2,1,0:T(8,128)(2,1)}) %all-gather.8.cloned.1.call-update) | async-done | bytes 1048592 | tf_op jit(solution)/shard_map/all_gather | solution.py:140
  196.7 3.1 %convolution_convert_fusion = bf16[512,512]{1,0:T(8,128)(2,1)} fusion(bf16[512,1024]{1,0:T(8,128)(2,1)} %bitcast.66, bf16[1,1024,512]{2,1,0:T(8,128)(2,1)} %param.35), kind=kOutput, calls=%fused_computation.30 | convolution fusion | flops 537133056 | bytes 2621440 | tf_op jit(solution)/shard_map/dot_general | solution.py:141
  199.8 4.6 %all-to-all-start.1 = ((bf16[8,64,512]{2,1,0:T(8,128)(2,1)}), bf16[8,64,512]{2,1,0:T(8,128)(2,1)S(1)}, u32[]{:S(2)}, u32[]{:S(2)}) async-start(bf16[8,64,512]{2,1,0:T(8,128)(2,1)} %bitcast.57), calls=%async_computation.2 | async-start | bytes 1048576 | tf_op jit(solution)/shard_map/all_to_all | solution.py:145
  204.4 0.1 copy.29
  204.5 15.2 %all-to-all-done.1 = bf16[8,64,512]{2,1,0:T(8,128)(2,1)S(1)} async-done(((bf16[8,64,512]{2,1,0:T(8,128)(2,1)}), bf16[8,64,512]{2,1,0:T(8,128)(2,1)S(1)}, u32[]{:S(2)}, u32[]{:S(2)}) %all-to-all-start.1) | async-done | bytes 524320 | tf_op jit(solution)/shard_map/all_to_all | solution.py:145
  219.7 1.2 gather_fusion.1
  220.9 0.3 reshape.190
  221.2 0.7 multiply_reduce_fusion
  221.9 0.7 add_convert_fusion
  (48 shorter events, 0.5 us)
Async XLA Ops:
  6.5 65.5 %copy-start = (bf16[512,2048]{1,0:T(8,128)(2,1)S(1)}, bf16[512,2048]{1,0:T(8,128)(2,1)}, u32[]{:S(2)}) copy-start(bf16[512,2048]{1,0:T(8,128)(2,1)} %param.28) | copy-start | bytes 6291460
  6.5 36.4 %all-gather.4.cloned.1.call-start = ((), (), s32[]{:S(2)}) async-start(), calls=%async_computation.3 | async-start | bytes 1179648 | tf_op jit(solution)/shard_map/all_gather | solution.py:81
  7.3 55.5 %all-gather.6.cloned.1.call-start = ((), (), s32[]{:S(2)}) async-start(), calls=%async_computation.4 | async-start | bytes 1179648 | tf_op jit(solution)/shard_map/all_gather | solution.py:82
  8.0 89.3 %reduce-scatter.2.cloned.1.call-start = ((), (), s32[]{:S(2)}) async-start(), calls=%async_computation.5 | async-start | bytes 655360 | tf_op jit(solution)/shard_map/reduce_scatter | solution.py:106
  65.4 1.2 copy-start.6
  65.4 1.2 copy-start.9
  65.4 1.2 copy-start.10
  66.6 1.4 copy-start.2
  72.0 2.2 copy-start.4
  72.0 25.3 %copy-start.1 = (bf16[32,2048]{1,0:T(8,128)(2,1)S(1)}, bf16[32,2048]{1,0:T(8,128)(2,1)}, u32[]{:S(2)}) copy-start(bf16[32,2048]{1,0:T(8,128)(2,1)} %param.29) | copy-start | bytes 393220
  72.0 27.5 %copy-start.3 = (f32[2048]{0:T(1024)S(1)}, f32[2048]{0:T(1024)}, u32[]{:S(2)}) copy-start(f32[2048]{0:T(1024)} %param.30) | copy-start | bytes 24580
  73.3 123.4 %all-gather.8.cloned.1.call-start = ((), (), s32[]{:S(2)}) async-start(), calls=%async_computation.6 | async-start | bytes 1310720 | tf_op jit(solution)/shard_map/all_gather | solution.py:140
  115.9 53.6 %copy-start.7 = (bf16[1,2048,256]{2,1,0:T(8,128)(2,1)S(1)}, bf16[1,2048,256]{2,1,0:T(8,128)(2,1)}, u32[]{:S(2)}) copy-start(bf16[1,2048,256]{2,1,0:T(8,128)(2,1)} %param.33) | copy-start | bytes 3145732
  169.5 1.2 copy-start.8
  196.7 7.7 %copy-start.5 = (f32[128,2]{0,1:T(2,128)S(1)}, f32[128,2]{0,1:T(2,128)}, u32[]{:S(2)}) copy-start(f32[128,2]{0,1:T(2,128)} %param.32) | copy-start | bytes 3076
  199.8 19.9 %all-to-all-start.1 = ((bf16[8,64,512]{2,1,0:T(8,128)(2,1)}), bf16[8,64,512]{2,1,0:T(8,128)(2,1)S(1)}, u32[]{:S(2)}, u32[]{:S(2)}) async-start(bf16[8,64,512]{2,1,0:T(8,128)(2,1)} %bitcast.57), calls=%async_computation.2 | async-start | bytes 1048576 | tf_op jit(solution)/shard_map/all_to_all | solution.py:145
Sparse Core Ops, SparseCore 0:
  8.9 27.7 all-gather.3
  38.3 24.4 all-gather.5
  73.5 23.8 reduce-scatter.1
  172.3 24.3 all-gather.7
where the time goes:
time: 230 us; the launch traced here: 229 us
  blocking collectives  96.1 us (42%)
  waiting for transfers between devices  80.3 us (35%)
  between operations  13.3 us (6%)
  local copies, waits for them, and re-layouts  13.2 us (6%)
  matrix products  12.4 us (5%)
  other arithmetic  9.06 us (4%)
  starting transfers between devices  4.73 us (2%)
    all_to_all x1, blocking collectives, per_device(): rows = lax.all_to_all(send, 'sp', split_axis=0, concat_axis=0, tiled=True)  53.6 us
    all_gather x1, waiting for transfers between devices, per_device(): hidden_all = lax.all_gather(hidden, 'tp', axis=2, tiled=True)  24.5 us
    all_gather x1, waiting for transfers between devices, per_device(): vals_b = lax.all_gather(value_b, 'sp', axis=1, tiled=True)  19.9 us
    reduce_scatter x1, waiting for transfers between devices, per_device(): lax.psum_scatter((term + lax.dot_general(attn_b, out_weight_b, (((0,), (0...  19.3 us
    all_gather x1, blocking collectives, per_device(): keys_a = lax.all_gather(key_a, 'sp', axis=1, tiled=True)  17.6 us
    all_to_all x1, waiting for transfers between devices, per_device(): lax.all_to_all(result, 'sp', split_axis=0, concat_axis=0, tiled=True)  15.2 us
    all_gather x1, blocking collectives, per_device(): vals_a = lax.all_gather(value_a, 'sp', axis=1, tiled=True)  14.7 us
    all_gather x1, blocking collectives, per_device(): normed_all = lax.all_gather(normed, 'tp', axis=0, tiled=True)  10.2 us
  transfers between devices with their start and end apart: 5, of which 4 were waited for; matrix products, arithmetic and copies ran while one was open for 3% of the time, Pallas kernels for 0%

commit v1 on v0

--- a/solution.py
+++ b/solution.py
@@ -1,6 +1,10 @@
+import functools
+
 import jax
 import jax.numpy as jnp
 from jax import lax
+from jax.experimental import pallas as pl
+from jax.experimental.pallas import tpu as pltpu
 from jax.sharding import PartitionSpec as P
 
 HDA = 64
@@ -151,6 +155,465 @@
     return (own_cols.astype(jnp.float32) + routed).astype(jnp.bfloat16)
 
 
+MESH = pl.DeviceIdType.MESH
+F32 = jnp.float32
+BF16 = jnp.bfloat16
+
+
+def fused_kernel(
+    dims,
+    q_a, k_a, v_a, cum_a, q_b, k_b, v_b, cum_b, residual, gain, ids, route,
+    wa_hbm, wb_hbm, gate_hbm, up_hbm, down_hbm,
+    out,
+    wa, wb, gw, uw, dw,
+    got_a, got_b, cols, mine_a, mine_b, att_a, att_b,
+    ps, rs, nb, nf, onehot, wsend, wgot, dsend, xs, hid, own, part_send, part_got, ret_send, ret,
+    w_sem, qkv_send, qkv_recv, att_send, att_recv, rs_send, rs_recv, nf_send, nf_recv,
+    ws_send, ws_recv, d_send, d_recv, ag_send, ag_recv, pair_send, pair_recv,
+    h_send, h_recv, e_send, e_recv, r_send, r_recv,
+):
+    n_sp, n_tp, heads_a, da, db, group_size = dims
+    s = lax.axis_index("sp")
+    t = lax.axis_index("tp")
+    z = s // 2
+    c = s % 2
+    nz = n_sp // 2
+    tok = q_a.shape[1]
+    groups = nz
+    slots = dsend.shape[1]
+    sub = tok // n_tp
+    feat = nf.shape[1]
+
+    def tp_to(j):
+        if n_tp == 4:
+            return {1: t + 1 - 2 * (t % 2), 2: (t + 2) % 4, 3: 3 - t}[j]
+        return (t + j) % n_tp
+
+    def tp_from(j):
+        if n_tp == 4:
+            return tp_to(j)
+        return (t + n_tp - j) % n_tp
+
+    def remote(src, dst, send, recv, sp, tp):
+        return pltpu.make_async_remote_copy(
+            src_ref=src, dst_ref=dst, send_sem=send, recv_sem=recv,
+            device_id={"sp": sp, "tp": tp}, device_id_type=MESH,
+        )
+
+    loads = []
+    for i, (src, dst) in enumerate(
+        ((wa_hbm, wa), (wb_hbm, wb), (gate_hbm.at[0], gw), (up_hbm.at[0], uw), (down_hbm.at[0], dw))
+    ):
+        copy = pltpu.make_async_copy(src, dst, w_sem.at[i])
+        copy.start()
+        loads.append(copy)
+
+    barrier = pltpu.get_barrier_semaphore()
+    for k in range(1, n_sp):
+        pl.semaphore_signal(
+            barrier, inc=1, device_id={"sp": (s + k) % n_sp, "tp": t}, device_id_type=MESH
+        )
+    for j in range(1, n_tp):
+        pl.semaphore_signal(
+            barrier, inc=1, device_id={"sp": s, "tp": tp_to(j)}, device_id_type=MESH
+        )
+    pl.semaphore_wait(barrier, n_sp - 1 + n_tp - 1)
+
+    sources = ((q_a, k_a, v_a), (q_b, k_b, v_b))
+    got = (got_a, got_b)
+    sizes = (da, db)
+
+    def qkv_copies(core):
+        copies = []
+        for k in range(1, n_sp):
+            target = (s + k) % n_sp
+            kind = (core + k) % 2
+            d = sizes[kind]
+            rows = pl.ds(pl.multiple_of((target // 2) * d, d), d)
+            for m in range(3):
+                copies.append(remote(
+                    sources[kind][m].at[rows], got[kind].at[m, s],
+                    qkv_send.at[m, k], qkv_recv.at[m, s], target, t,
+                ))
+        return copies
+
+    for core in range(2):
+        @pl.when(c == core)
+        def _(core=core):
+            for copy in qkv_copies(core):
+                copy.start()
+            d = sizes[core]
+            rows = pl.ds(pl.multiple_of(z * d, d), d)
+            for m in range(3):
+                got[core][m, s] = sources[core][m][rows, :]
+
+    ids_v = ids[...].astype(F32)
+    id0 = ids_v[:, 0:1]
+    lane = lax.broadcasted_iota(jnp.int32, (tok, 128), 1).astype(F32)
+    first = lane * group_size
+    member = (id0 >= first) & (id0 < first + group_size) & (lane < groups)
+    member = jnp.where(member, 1.0, 0.0)
+    low = lax.broadcasted_iota(jnp.int32, (tok, tok), 1) < lax.broadcasted_iota(jnp.int32, (tok, tok), 0)
+    rank = jnp.dot(
+        jnp.where(low, 1.0, 0.0).astype(BF16), member.astype(BF16), preferred_element_type=F32
+    )
+    slot = jnp.sum(member * (rank + lane * slots), axis=1, keepdims=True)
+    base = jnp.sum(member * first, axis=1, keepdims=True)
+    wide = lax.broadcasted_iota(jnp.int32, (tok, groups * slots), 1).astype(F32)
+    pick = jnp.where(wide == slot, 1.0, 0.0)
+    onehot[...] = pick.astype(BF16)
+    spread = jnp.transpose(pick).astype(BF16)
+    even = id0 == base
+    r0 = route[:, 0:1]
+    r1 = route[:, 1:2]
+    w_even = jnp.where(even, r0, r1)
+    w_odd = jnp.where(even, r1, r0)
+    w_lanes = jnp.where(lane == 0.0, w_even, jnp.where(lane == 1.0, w_odd, 0.0))
+    hi = w_lanes.astype(BF16)
+    rest = w_lanes - hi.astype(F32)
+    mid = rest.astype(BF16)
+    tail = (rest - mid.astype(F32)).astype(BF16)
+    w_slots = (
+        jnp.dot(spread, hi, preferred_element_type=F32)
+        + jnp.dot(spread, mid, preferred_element_type=F32)
+        + jnp.dot(spread, tail, preferred_element_type=F32)
+    )
+    wsend[...] = w_slots.reshape(groups, slots, 128)
+    wgot[z] = wsend[z]
+    w_copies = []
+    for k in range(1, nz):
+        zt = (z + k) % nz
+        copy = remote(wsend.at[zt], wgot.at[z], ws_send.at[k], ws_recv.at[k], 2 * zt + c, t)
+        copy.start()
+        w_copies.append(copy)
+
+    span = 2 * tok
+    mine = (mine_a, mine_b)
+    att = (att_a, att_b)
+    cums = (cum_a, cum_b)
+
+    def att_copy(core, dest):
+        d = sizes[core]
+        rows = pl.ds(pl.multiple_of(z * d, d), d)
+        return remote(
+            mine[core].at[dest], att[core].at[rows], att_send.at[dest], att_recv.at[s], dest, t
+        )
+
+    def attend(core):
+        d = sizes[core]
+        ref = got[core]
+        row = cums[core][pl.ds(z, 1), :]
+        for j in range(n_sp):
+            part = row[:, j * tok:(j + 1) * tok]
+            cols[pl.ds(j * tok, tok), :] = jnp.transpose(jnp.broadcast_to(part, (tok, tok)))
+        scale = d ** (-0.5)
+        keys_t = []
+        values = []
+        for step in range(n_sp // 2):
+            for src in (2 * step, 2 * step + 1):
+                @pl.when(s != src)
+                def _(src=src):
+                    for m in range(3):
+                        remote(
+                            ref.at[m, src], ref.at[m, src],
+                            qkv_send.at[m, 0], qkv_recv.at[m, src], src, t,
+                        ).wait_recv()
+            for src in (2 * step, 2 * step + 1):
+                keys_t.append(jnp.transpose(ref[1, src]))
+                values.append(ref[2, src])
+            queries = jnp.concatenate([ref[0, 2 * step], ref[0, 2 * step + 1]], axis=1)
+            count = span * (step + 1)
+            keys = jnp.concatenate(keys_t, axis=0)
+            vals = jnp.concatenate(values, axis=1)
+            score = jnp.dot(keys, queries, preferred_element_type=F32) * scale
+            cum_k = cols[pl.ds(0, count), :]
+            cum_q = row[:, step * span:(step + 1) * span]
+            score = score + (cum_q - jnp.concatenate([cum_k, cum_k], axis=1))
+            k_at = lax.broadcasted_iota(jnp.int32, (count, span), 0)
+            q_at = lax.broadcasted_iota(jnp.int32, (count, span), 1) + step * span
+            score = jnp.where(k_at <= q_at, score, -jnp.inf)
+            best = jnp.max(score, axis=0, keepdims=True)
+            weight = jnp.exp(score - best)
+            total = jnp.sum(weight, axis=0, keepdims=True)
+            res = jnp.dot(vals, weight.astype(BF16), preferred_element_type=F32) / total
+            res = res.astype(BF16)
+            for half in range(2):
+                dest = 2 * step + half
+                mine[core][dest] = res[:, half * tok:(half + 1) * tok]
+
+                @pl.when(s != dest)
+                def _(dest=dest):
+                    att_copy(core, dest).start()
+
+                @pl.when(s == dest)
+                def _(dest=dest):
+                    att[core][pl.ds(pl.multiple_of(z * d, d), d), :] = mine[core][dest]
+
+    for core in range(2):
+        @pl.when(c == core)
+        def _(core=core):
+            attend(core)
+
+    for src in range(n_sp):
+        core = src % 2
+        d = sizes[core]
+
+        @pl.when(s != src)
+        def _(src=src, core=core, d=d):
+            part = att[core].at[pl.ds((src // 2) * d, d)]
+            remote(part, part, att_send.at[src], att_recv.at[src], src, t).wait_recv()
+
+    loads[0].wait()
+    loads[1].wait()
+    left_a = jnp.transpose(att_a[...])
+    left_b = jnp.transpose(att_b[...])
+    pieces = ps.shape[0]
+    width = ps.shape[2]
+    rs_copies = []
+    for ch in range(pieces):
+        at = pl.ds(ch * width, width)
+        term = jnp.dot(left_a, wa[:, at], preferred_element_type=F32)
+        term = term + jnp.dot(left_b, wb[:, at], preferred_element_type=F32)
+        ps[ch] = term.astype(BF16)
+        for j in range(1, n_tp):
+            to = tp_to(j)
+            copy = remote(
+                ps.at[ch, pl.ds(pl.multiple_of(to * sub, sub), sub)], rs.at[ch, j - 1],
+                rs_send.at[ch, j - 1], rs_recv.at[ch, j - 1], s, to,
+            )
+            copy.start()
+            rs_copies.append(copy)
+    sums = []
+    for ch in range(pieces):
+        at = pl.ds(ch * width, width)
+        value = residual[:, at].astype(F32) + ps[
+            ch, pl.ds(pl.multiple_of(t * sub, sub), sub), :
+        ].astype(F32)
+        for j in range(1, n_tp):
+            rs_copies[ch * (n_tp - 1) + j - 1].wait_recv()
+            value = value + rs[ch, j - 1].astype(F32)
+        sums.append(value)
+    summed = jnp.concatenate(sums, axis=1)
+    center = summed - jnp.mean(summed, axis=-1, keepdims=True)
+    variance = jnp.mean(center * center, axis=-1, keepdims=True)
+    normed = (center * lax.rsqrt(variance + norm_eps) * gain[...]).astype(BF16)
+    for i in range(n_tp):
+        nb[i] = normed[:, i * feat:(i + 1) * feat]
+    here = pl.ds(pl.multiple_of(t * sub, sub), sub)
+    nf_copies = []
+    for j in range(1, n_tp):
+        to = tp_to(j)
+        copy = remote(nb.at[to], nf.at[here], nf_send.at[j - 1], nf_recv.at[j - 1], s, to)
+        copy.start()
+        nf_copies.append(copy)
+    nf[here, :] = nb[t]
+    for copy in nf_copies:
+        copy.wait_recv()
+
+    spread = jnp.transpose(onehot[...].astype(F32)).astype(BF16)
+    dsend[...] = jnp.dot(spread, nf[...], preferred_element_type=F32).astype(BF16).reshape(
+        groups, slots, feat
+    )
+    d_copies = []
+    for k in range(1, nz):
+        zt = (z + k) % nz
+        copy = remote(dsend.at[zt], xs.at[c, t, z], d_send.at[k], d_recv.at[k], 2 * zt + c, t)
+        copy.start()
+        d_copies.append(copy)
+    xs[c, t, z] = dsend[z]
+    mate = 2 * z + 1 - c
+    ag_copies = []
+    pair_copies = []
+    for k in range(nz):
+        zs = (z + nz - k) % nz
+        if k:
+            d_copies[k - 1].wait_recv()
+        block = xs.at[c, t, zs]
+        row = []
+        for j in range(1, n_tp):
+            copy = remote(block, block, ag_send.at[j - 1, k], ag_recv.at[j - 1, k], s, tp_to(j))
+            copy.start()
+            row.append(copy)
+        ag_copies.append(row)
+        copy = remote(block, block, pair_send.at[0, k], pair_recv.at[0, k], mate, t)
+        copy.start()
+        pair_copies.append([copy])
+
+    loads[2].wait()
+    loads[3].wait()
+    h_copies = []
+    for k in range(nz):
+        zs = (z + nz - k) % nz
+        for j in range(1, n_tp):
+            ag_copies[k][j - 1].wait_recv()
+            block = xs.at[c, tp_from(j), zs]
+            copy = remote(block, block, pair_send.at[j, k], pair_recv.at[j, k], mate, t)
+            copy.start()
+            pair_copies[k].append(copy)
+        for j in range(n_tp):
+            pair_copies[k][j].wait_recv()
+        rows = [
+            jnp.concatenate([xs[0, i, zs], xs[1, i, zs]], axis=0) for i in range(n_tp)
+        ]
+        rows = jnp.concatenate(rows, axis=1)
+        gate = jnp.dot(rows, gw[...], preferred_element_type=F32)
+        upper = jnp.dot(rows, uw[...], preferred_element_type=F32)
+        hid[zs, t] = (gate / (1.0 + jnp.exp(-gate)) * upper).astype(BF16)
+        block = hid.at[zs, t]
+        row = []
+        for j in range(1, n_tp):
+            copy = remote(block, block, h_send.at[j - 1, k], h_recv.at[j - 1, k], s, tp_to(j))
+            copy.start()
+            row.append(copy)
+        h_copies.append(row)
+
+    loads[4].wait()
+    e_copies = []
+    for k in range(nz):
+        zs = (z + nz - k) % nz
+        for copy in h_copies[k]:
+            copy.wait_recv()
+        rows = jnp.concatenate([hid[zs, i] for i in range(n_tp)], axis=1)
+        result = jnp.dot(rows, dw[...], preferred_element_type=F32)
+        top = result[:slots]
+        bottom = result[slots:]
+        own[zs] = jnp.where(c == 0, top, bottom)
+        part_send[zs] = jnp.where(c == 0, bottom, top).astype(BF16)
+        copy = remote(part_send.at[zs], part_got.at[zs], e_send.at[k], e_recv.at[k], mate, t)
+        copy.start()
+        e_copies.append(copy)
+
+    r_copies = []
+    for k in range(nz):
+        zs = (z + nz - k) % nz
+        if k:
+            w_copies[k - 1].wait_recv()
+        e_copies[k].wait_recv()
+        both = wgot[zs]
+        w0 = both[:, 0:1]
+        w1 = both[:, 1:2]
+        own_w = jnp.where(c == 0, w0, w1)
+        mate_w = jnp.where(c == 0, w1, w0)
+        total = (own_w * own[zs] + mate_w * part_got[zs].astype(F32)).astype(BF16)
+        if k:
+            ret_send[k] = total
+            copy = remote(
+                ret_send.at[k], ret.at[pl.ds(pl.multiple_of(z * slots, slots), slots)],
+                r_send.at[k], r_recv.at[k], 2 * zs + c, t,
+            )
+            copy.start()
+            r_copies.append(copy)
+        else:
+            ret[pl.ds(pl.multiple_of(z * slots, slots), slots), :] = total
+
+    for k in range(1, nz):
+        r_copies[k - 1].wait_recv()
+    routed = jnp.dot(onehot[...], ret[...], preferred_element_type=F32)
+    out[...] = (nf[...].astype(F32) + routed).astype(BF16)
+
+    for core in range(2):
+        @pl.when(c == core)
+        def _(core=core):
+            for copy in qkv_copies(core):
+                copy.wait_send()
+            for dest in range(n_sp):
+                @pl.when(s != dest)
+                def _(dest=dest):
+                    att_copy(core, dest).wait_send()
+    flat = w_copies + rs_copies + nf_copies + d_copies + e_copies + r_copies
+    for group in (ag_copies, pair_copies, h_copies):
+        for row in group:
+            flat = flat + row
+    for copy in flat:
+        copy.wait_send()
+
+
+def fused(
+    query_a, key_a, value_a, cumlog_a, query_b, key_b, value_b, cumlog_b, out_weight_a,
+    out_weight_b, residual, norm_gain, expert_ids, route_weight, gate_w, up_w, down_w,
+):
+    n_sp = lax.axis_size("sp")
+    n_tp = lax.axis_size("tp")
+    nz = n_sp // 2
+    tok = query_a.shape[1]
+    sub = tok // n_tp
+    model = residual.shape[1]
+    feat = down_w.shape[2]
+    inner = gate_w.shape[2]
+    group_size = n_sp // GROUPS
+    slots = tok // TOP
+    pieces = 2
+    width = model // pieces
+    dims = (n_sp, n_tp, cumlog_a.shape[0], HDA, HDB, group_size)
+    vmem = pl.BlockSpec(memory_space=pltpu.VMEM)
+    anyw = pl.BlockSpec(memory_space=pl.ANY)
+    dma = pltpu.SemaphoreType.DMA
+    scratch = [
+        pltpu.VMEM(out_weight_a.shape, BF16),
+        pltpu.VMEM(out_weight_b.shape, BF16),
+        pltpu.VMEM(gate_w.shape[1:], BF16),
+        pltpu.VMEM(up_w.shape[1:], BF16),
+        pltpu.VMEM(down_w.shape[1:], BF16),
+        pltpu.VMEM((3, n_sp, HDA, tok), BF16),
+        pltpu.VMEM((3, n_sp, HDB, tok), BF16),
+        pltpu.VMEM((n_sp * tok, tok), F32),
+        pltpu.VMEM((n_sp, HDA, tok), BF16),
+        pltpu.VMEM((n_sp, HDB, tok), BF16),
+        pltpu.VMEM(query_a.shape, BF16),
+        pltpu.VMEM(query_b.shape, BF16),
+        pltpu.VMEM((pieces, tok, width), BF16),
+        pltpu.VMEM((pieces, n_tp - 1, sub, width), BF16),
+        pltpu.VMEM((n_tp, sub, feat), BF16),
+        pltpu.VMEM((tok, feat), BF16),
+        pltpu.VMEM((tok, nz * slots), BF16),
+        pltpu.VMEM((nz, slots, 128), F32),
+        pltpu.VMEM((nz, slots, 128), F32),
+        pltpu.VMEM((nz, slots, feat), BF16),
+        pltpu.VMEM((2, n_tp, nz, slots, feat), BF16),
+        pltpu.VMEM((nz, n_tp, 2 * slots, inner), BF16),
+        pltpu.VMEM((nz, slots, feat), F32),
+        pltpu.VMEM((nz, slots, feat), BF16),
+        pltpu.VMEM((nz, slots, feat), BF16),
+        pltpu.VMEM((nz, slots, feat), BF16),
+        pltpu.VMEM((nz * slots, feat), BF16),
+        dma((5,)),
+        dma((3, n_sp)), dma((3, n_sp)),
+        dma((n_sp,)), dma((n_sp,)),
+        dma((pieces, n_tp - 1)), dma((pieces, n_tp - 1)),
+        dma((n_tp - 1,)), dma((n_tp - 1,)),
+        dma((nz,)), dma((nz,)),
+        dma((nz,)), dma((nz,)),
+        dma((n_tp - 1, nz)), dma((n_tp - 1, nz)),
+        dma((n_tp, nz)), dma((n_tp, nz)),
+        dma((n_tp - 1, nz)), dma((n_tp - 1, nz)),
+        dma((nz,)), dma((nz,)),
+        dma((nz,)), dma((nz,)),
+    ]
+    return pl.pallas_call(
+        functools.partial(fused_kernel, dims),
+        out_shape=jax.ShapeDtypeStruct((tok, feat), BF16),
+        in_specs=[vmem] * 12 + [anyw] * 5,
+        out_specs=vmem,
+        scratch_shapes=scratch,
+        compiler_params=pltpu.CompilerParams(
+            collective_id=0, has_side_effects=True, vmem_limit_bytes=48 * 1024 * 1024
+        ),
+    )(
+        query_a, key_a, value_a, cumlog_a, query_b, key_b, value_b, cumlog_b, residual,
+        norm_gain.reshape(1, -1), expert_ids, route_weight, out_weight_a, out_weight_b,
+        gate_w, up_w, down_w,
+    )
+
+
+def choose(*args):
+    n_sp = lax.axis_size("sp")
+    heads_a = args[3].shape[0]
+    heads_b = args[7].shape[0]
+    fits = heads_a == heads_b and heads_a + heads_b == n_sp
+    fits = fits and n_sp == GROUPS * TOP and n_sp == 2 * GROUPS
+    return (fused if fits else per_device)(*args)
+
+
 def solution(mesh):
     placed = (
         P("tp", "sp"),
@@ -172,5 +635,5 @@
         P("sp", None, "tp"),
     )
     return jax.shard_map(
-        per_device, mesh=mesh, in_specs=placed, out_specs=P("sp", "tp"), check_vma=False
-    )
+        choose, mesh=mesh, in_specs=placed, out_specs=P("sp", "tp"), check_vma=False
+    )

time: 230 us -> 91.4 us (0.40)
  blocking collectives: 96.1 us -> 0 us
  waiting for transfers between devices: 80.3 us -> 0 us
  Pallas kernels: 0 us -> 75.3 us
  between operations: 13.3 us -> 0.03 us
  matrix products: 12.4 us -> 0 us
  other arithmetic: 9.06 us -> 0 us
  starting transfers between devices: 4.73 us -> 0 us
    pallas_call x0 -> x1, Pallas kernels: none -> 75.3 us  [fused(): pl.pallas_call(functools.partial(fused_kernel, dims), out_shape=jax.Shape...]
    all_to_all x1 -> x0, blocking collectives: 53.6 us -> none  [per_device(): rows = lax.all_to_all(send, 'sp', split_axis=0, concat_axis=0, tiled=True)]
    all_gather x3 -> x0, waiting for transfers between devices: 44.4 us -> none  [the longest x1 24.5 us: per_device(): hidden_all = lax.all_gather(hidden, 'tp', axis=2, tiled=True)]
    all_gather x3 -> x0, blocking collectives: 42.5 us -> none  [the longest x1 17.6 us: per_device(): keys_a = lax.all_gather(key_a, 'sp', axis=1, tiled=True)]
    reduce_scatter x1 -> x0, waiting for transfers between devices: 19.3 us -> none  [per_device(): lax.psum_scatter((term + lax.dot_general(attn_b, out_weight_b, (((0,), (0...]
    all_to_all x1 -> x0, waiting for transfers between devices: 15.2 us -> none  [per_device(): lax.all_to_all(result, 'sp', split_axis=0, concat_axis=0, tiled=True)]
    unnamed x16 -> x31, local copies, waits for them, and re-layouts: 1.44 us -> 15.4 us
    dot_general x9 -> x0, matrix products: 12.4 us -> none  [the longest x1 3.08 us: per_device(): jnp.dot(hidden_all.reshape(sources * items, -1), down_w[0], preferred_ele...]
  transfers between devices with their start and end apart: 5 -> 0, of which waited for: 4 -> 0; matrix products, arithmetic and copies ran while one was open for 3% -> 0% of each run, Pallas kernels for 0% -> 0%
where the time goes in v1:
time: 91.4 us; the launch traced here: 90.7 us
  Pallas kernels  75.3 us (82%)
  local copies, waits for them, and re-layouts  15.4 us (17%)
    pallas_call x1, Pallas kernels, fused(): pl.pallas_call(functools.partial(fused_kernel, dims), out_shape=jax.Shape...  75.3 us
    unnamed x31, local copies, waits for them, and re-layouts  15.4 us

profile of v1, /device:TPU:0, one launch (start us, length us, event | category | flops | bytes accessed | tf_op | source)
XLA Modules:
  0.0 90.7 jit_solution(4213433374923320654)
XLA Ops:
  0.0 0.8 copy.18.ids
  0.8 0.8 copy.19.route
  1.6 0.0 copy-start
  1.6 1.2 %copy-done = bf16[256,2048]{1,0:T(8,128)(2,1)S(1)} copy-done((bf16[256,2048]{1,0:T(8,128)(2,1)S(1)}, bf16[256,2048]{1,0:T(8,128)(2,1)}, u32[]{:S(2)}) %copy-start) | copy-done | bytes 1048600
  2.8 0.0 copy-start.1
  2.8 1.2 %copy-done.1 = bf16[1,2048,256]{2,1,0:T(8,128)(2,1)S(1)} copy-done((bf16[1,2048,256]{2,1,0:T(8,128)(2,1)S(1)}, bf16[1,2048,256]{2,1,0:T(8,128)(2,1)}, u32[]{:S(2)}) %copy-start.1) | copy-done | bytes 1048600
  4.0 0.0 copy-start.2
  4.0 1.2 %copy-done.2 = bf16[1,2048,256]{2,1,0:T(8,128)(2,1)S(1)} copy-done((bf16[1,2048,256]{2,1,0:T(8,128)(2,1)S(1)}, bf16[1,2048,256]{2,1,0:T(8,128)(2,1)}, u32[]{:S(2)}) %copy-start.2) | copy-done | bytes 1048600
  5.2 0.0 copy-start.3
  5.2 1.2 %copy-done.3 = bf16[1,1024,512]{2,1,0:T(8,128)(2,1)S(1)} copy-done((bf16[1,1024,512]{2,1,0:T(8,128)(2,1)S(1)}, bf16[1,1024,512]{2,1,0:T(8,128)(2,1)}, u32[]{:S(2)}) %copy-start.3) | copy-done | bytes 1048600
  6.5 0.0 copy-start.4
  6.5 0.9 copy-done.4
  7.4 0.0 copy-start.5
  7.4 0.9 copy-done.5
  8.3 0.0 copy-start.6
  8.3 0.9 copy-done.6
  9.2 0.0 copy-start.7
  9.2 0.9 copy-done.7
  10.1 0.0 copy-start.8
  10.1 0.8 copy-done.8
  10.9 0.0 copy-start.9
  10.9 0.8 copy-done.9
  11.8 0.0 copy-start.10
  11.8 0.8 copy-done.10
  12.6 0.0 copy-start.11
  12.6 0.7 copy-done.11
  13.3 0.0 copy-start.12
  13.3 0.7 copy-done.12
  14.0 0.0 copy-start.13
  14.0 0.7 copy-done.13
  14.7 75.3 %shard_map.163 = bf16[128,512]{1,0:T(8,128)(2,1)S(1)} custom-call(bf16[256,128]{1,0:T(8,128)(2,1)S(1)} %copy-done.8, bf16[256,128]{1,0:T(8,128)(2,1)S(1)} %copy-done.9, bf16[256,128]{1,0:T(8,128)(2,1)S(1)} %copy-done.10, f32[4,1024]{1,0:T(4,128)S(1)} %copy-done.11, bf16[512,128]{1,0:T(8,128)(2,1)S(1)} %copy-done.4, bf16[512,128]{1,0:T(8,128)(2,1)S(1)} %copy-done.5, ...), custom_call_target="tpu_custom_call" | custom-call | tf_op jit(solution)/shard_map/pallas_call | solution.py:592
  90.1 0.7 copy.21
Async XLA Ops:
  1.6 1.2 %copy-start = (bf16[256,2048]{1,0:T(8,128)(2,1)S(1)}, bf16[256,2048]{1,0:T(8,128)(2,1)}, u32[]{:S(2)}) copy-start(bf16[256,2048]{1,0:T(8,128)(2,1)} %wa_hbm.1) | copy-start | bytes 3145732
  2.8 1.2 %copy-start.1 = (bf16[1,2048,256]{2,1,0:T(8,128)(2,1)S(1)}, bf16[1,2048,256]{2,1,0:T(8,128)(2,1)}, u32[]{:S(2)}) copy-start(bf16[1,2048,256]{2,1,0:T(8,128)(2,1)} %gate_hbm.1) | copy-start | bytes 3145732
  4.0 1.2 %copy-start.2 = (bf16[1,2048,256]{2,1,0:T(8,128)(2,1)S(1)}, bf16[1,2048,256]{2,1,0:T(8,128)(2,1)}, u32[]{:S(2)}) copy-start(bf16[1,2048,256]{2,1,0:T(8,128)(2,1)} %up_hbm.1) | copy-start | bytes 3145732
  5.2 1.2 %copy-start.3 = (bf16[1,1024,512]{2,1,0:T(8,128)(2,1)S(1)}, bf16[1,1024,512]{2,1,0:T(8,128)(2,1)}, u32[]{:S(2)}) copy-start(bf16[1,1024,512]{2,1,0:T(8,128)(2,1)} %down_hbm.1) | copy-start | bytes 3145732
  6.5 0.9 copy-start.4
  7.4 0.9 copy-start.5
  8.3 0.9 copy-start.6
  9.2 0.9 copy-start.7
  10.1 0.8 copy-start.8
  10.9 0.8 copy-start.9
  11.8 0.8 copy-start.10
  12.6 0.7 copy-start.11
  13.3 0.7 copy-start.12
  14.0 0.7 copy-start.13

commit v2 on v1

--- a/solution.py
+++ b/solution.py
@@ -162,9 +162,11 @@
 
 def fused_kernel(
     dims,
-    q_a, k_a, v_a, cum_a, q_b, k_b, v_b, cum_b, residual, gain, ids, route,
+    q_a_hbm, k_a_hbm, v_a_hbm, cum_a_hbm, q_b_hbm, k_b_hbm, v_b_hbm, cum_b_hbm,
+    residual_hbm, gain_hbm, ids_hbm, route_hbm,
     wa_hbm, wb_hbm, gate_hbm, up_hbm, down_hbm,
     out,
+    q_a, k_a, v_a, cum_a, q_b, k_b, v_b, cum_b, residual, gain, ids, route,
     wa, wb, gw, uw, dw,
     got_a, got_b, cols, mine_a, mine_b, att_a, att_b,
     ps, rs, nb, nf, onehot, wsend, wgot, dsend, xs, hid, own, part_send, part_got, ret_send, ret,
@@ -202,7 +204,13 @@
 
     loads = []
     for i, (src, dst) in enumerate(
-        ((wa_hbm, wa), (wb_hbm, wb), (gate_hbm.at[0], gw), (up_hbm.at[0], uw), (down_hbm.at[0], dw))
+        (
+            (q_a_hbm, q_a), (k_a_hbm, k_a), (v_a_hbm, v_a),
+            (q_b_hbm, q_b), (k_b_hbm, k_b), (v_b_hbm, v_b),
+            (ids_hbm, ids), (route_hbm, route), (cum_a_hbm, cum_a), (cum_b_hbm, cum_b),
+            (wa_hbm, wa), (wb_hbm, wb), (residual_hbm, residual), (gain_hbm, gain),
+            (gate_hbm.at[0], gw), (up_hbm.at[0], uw), (down_hbm.at[0], dw),
+        )
     ):
         copy = pltpu.make_async_copy(src, dst, w_sem.at[i])
         copy.start()
@@ -219,6 +227,8 @@
         )
     pl.semaphore_wait(barrier, n_sp - 1 + n_tp - 1)
 
+    for copy in loads[:6]:
+        copy.wait()
     sources = ((q_a, k_a, v_a), (q_b, k_b, v_b))
     got = (got_a, got_b)
     sizes = (da, db)
@@ -247,8 +257,13 @@
             for m in range(3):
                 got[core][m, s] = sources[core][m][rows, :]
 
-    ids_v = ids[...].astype(F32)
-    id0 = ids_v[:, 0:1]
+    loads[6].wait()
+    loads[7].wait()
+
+    def upright(row):
+        return jnp.transpose(jnp.broadcast_to(row, (128, tok)))
+
+    id0 = upright(ids[0:1, :].astype(F32))
     lane = lax.broadcasted_iota(jnp.int32, (tok, 128), 1).astype(F32)
     first = lane * group_size
     member = (id0 >= first) & (id0 < first + group_size) & (lane < groups)
@@ -264,8 +279,8 @@
     onehot[...] = pick.astype(BF16)
     spread = jnp.transpose(pick).astype(BF16)
     even = id0 == base
-    r0 = route[:, 0:1]
-    r1 = route[:, 1:2]
+    r0 = upright(route[0:1, :])
+    r1 = upright(route[1:2, :])
     w_even = jnp.where(even, r0, r1)
     w_odd = jnp.where(even, r1, r0)
     w_lanes = jnp.where(lane == 0.0, w_even, jnp.where(lane == 1.0, w_odd, 0.0))
@@ -302,6 +317,7 @@
     def attend(core):
         d = sizes[core]
         ref = got[core]
+        loads[8 + core].wait()
         row = cums[core][pl.ds(z, 1), :]
         for j in range(n_sp):
             part = row[:, j * tok:(j + 1) * tok]
@@ -363,8 +379,8 @@
             part = att[core].at[pl.ds((src // 2) * d, d)]
             remote(part, part, att_send.at[src], att_recv.at[src], src, t).wait_recv()
 
-    loads[0].wait()
-    loads[1].wait()
+    for copy in loads[10:14]:
+        copy.wait()
     left_a = jnp.transpose(att_a[...])
     left_b = jnp.transpose(att_b[...])
     pieces = ps.shape[0]
@@ -439,8 +455,8 @@
         copy.start()
         pair_copies.append([copy])
 
-    loads[2].wait()
-    loads[3].wait()
+    loads[14].wait()
+    loads[15].wait()
     h_copies = []
     for k in range(nz):
         zs = (z + nz - k) % nz
@@ -467,7 +483,7 @@
             row.append(copy)
         h_copies.append(row)
 
-    loads[4].wait()
+    loads[16].wait()
     e_copies = []
     for k in range(nz):
         zs = (z + nz - k) % nz
@@ -514,6 +530,7 @@
     for core in range(2):
         @pl.when(c == core)
         def _(core=core):
+            loads[9 - core].wait()
             for copy in qkv_copies(core):
                 copy.wait_send()
             for dest in range(n_sp):
@@ -549,6 +566,18 @@
     anyw = pl.BlockSpec(memory_space=pl.ANY)
     dma = pltpu.SemaphoreType.DMA
     scratch = [
+        pltpu.VMEM(query_a.shape, BF16),
+        pltpu.VMEM(key_a.shape, BF16),
+        pltpu.VMEM(value_a.shape, BF16),
+        pltpu.VMEM(cumlog_a.shape, F32),
+        pltpu.VMEM(query_b.shape, BF16),
+        pltpu.VMEM(key_b.shape, BF16),
+        pltpu.VMEM(value_b.shape, BF16),
+        pltpu.VMEM(cumlog_b.shape, F32),
+        pltpu.VMEM(residual.shape, BF16),
+        pltpu.VMEM((1, model), F32),
+        pltpu.VMEM((TOP, tok), jnp.int32),
+        pltpu.VMEM((TOP, tok), F32),
         pltpu.VMEM(out_weight_a.shape, BF16),
         pltpu.VMEM(out_weight_b.shape, BF16),
         pltpu.VMEM(gate_w.shape[1:], BF16),
@@ -576,7 +605,7 @@
         pltpu.VMEM((nz, slots, feat), BF16),
         pltpu.VMEM((nz, slots, feat), BF16),
         pltpu.VMEM((nz * slots, feat), BF16),
-        dma((5,)),
+        dma((17,)),
         dma((3, n_sp)), dma((3, n_sp)),
         dma((n_sp,)), dma((n_sp,)),
         dma((pieces, n_tp - 1)), dma((pieces, n_tp - 1)),
@@ -592,15 +621,15 @@
     return pl.pallas_call(
         functools.partial(fused_kernel, dims),
         out_shape=jax.ShapeDtypeStruct((tok, feat), BF16),
-        in_specs=[vmem] * 12 + [anyw] * 5,
+        in_specs=[anyw] * 17,
         out_specs=vmem,
         scratch_shapes=scratch,
         compiler_params=pltpu.CompilerParams(
-            collective_id=0, has_side_effects=True, vmem_limit_bytes=48 * 1024 * 1024
+            collective_id=0, has_side_effects=True, vmem_limit_bytes=67043328
         ),
     )(
         query_a, key_a, value_a, cumlog_a, query_b, key_b, value_b, cumlog_b, residual,
-        norm_gain.reshape(1, -1), expert_ids, route_weight, out_weight_a, out_weight_b,
+        norm_gain.reshape(1, -1), expert_ids.T, route_weight.T, out_weight_a, out_weight_b,
         gate_w, up_w, down_w,
     )
 

time: 91.4 us -> 77.4 us (0.85)
  local copies, waits for them, and re-layouts: 15.4 us -> 1.57 us
    unnamed x31 -> x1, local copies, waits for them, and re-layouts: 15.4 us -> 1.57 us
where the time goes in v2:
time: 77.4 us; the launch traced here: 77.3 us
  Pallas kernels  75.7 us (98%)
  local copies, waits for them, and re-layouts  1.57 us (2%)
    pallas_call x1, Pallas kernels, fused(): pl.pallas_call(functools.partial(fused_kernel, dims), out_shape=jax.Shape...  75.7 us
    unnamed x1, local copies, waits for them, and re-layouts  1.57 us

profile of v2, /device:TPU:0, one launch (start us, length us, event | category | flops | bytes accessed | tf_op | source)
XLA Modules:
  0.0 77.3 jit_solution(10087345446403333954)
XLA Ops:
  0.0 75.7 %shard_map.163 = bf16[128,512]{1,0:T(8,128)(2,1)} custom-call(bf16[256,128]{1,0:T(8,128)(2,1)} %q_a_hbm.1, bf16[256,128]{1,0:T(8,128)(2,1)} %k_a_hbm.1, bf16[256,128]{1,0:T(8,128)(2,1)} %v_a_hbm.1, f32[4,1024]{1,0:T(4,128)} %cum_a_hbm.1, bf16[512,128]{1,0:T(8,128)(2,1)} %q_b_hbm.1, bf16[512,128]{1,0:T(8,128)(2,1)} %k_b_hbm.1, bf16[512,128]{1,0:T(8,128)(2,1)} %v_b_hbm.1, ...), custom_call_target="tpu_custom_call" | custom-call | tf_op jit(solution)/shard_map/pallas_call | solution.py:621
  75.7 1.6 %copy.19 = bf16[128,512]{1,0:T(8,128)(2,1)} copy(bf16[128,512]{1,0:T(8,128)(2,1)} %shard_map.163) | data formatting | bytes 262144

commit v3 on v2

--- a/solution.py
+++ b/solution.py
@@ -166,7 +166,7 @@
     residual_hbm, gain_hbm, ids_hbm, route_hbm,
     wa_hbm, wb_hbm, gate_hbm, up_hbm, down_hbm,
     out,
-    q_a, k_a, v_a, cum_a, q_b, k_b, v_b, cum_b, residual, gain, ids, route,
+    pack_a, cum_a, pack_b, cum_b, residual, gain, ids, route,
     wa, wb, gw, uw, dw,
     got_a, got_b, cols, mine_a, mine_b, att_a, att_b,
     ps, rs, nb, nf, onehot, wsend, wgot, dsend, xs, hid, own, part_send, part_got, ret_send, ret,
@@ -180,21 +180,14 @@
     z = s // 2
     c = s % 2
     nz = n_sp // 2
-    tok = q_a.shape[1]
+    tok = pack_a.shape[3]
     groups = nz
     slots = dsend.shape[1]
     sub = tok // n_tp
     feat = nf.shape[1]
 
     def tp_to(j):
-        if n_tp == 4:
-            return {1: t + 1 - 2 * (t % 2), 2: (t + 2) % 4, 3: 3 - t}[j]
-        return (t + j) % n_tp
-
-    def tp_from(j):
-        if n_tp == 4:
-            return tp_to(j)
-        return (t + n_tp - j) % n_tp
+        return (t + 1 - 2 * (t % 2), (t + 2) % 4, 3 - t)[j - 1]
 
     def remote(src, dst, send, recv, sp, tp):
         return pltpu.make_async_remote_copy(
@@ -205,8 +198,8 @@
     loads = []
     for i, (src, dst) in enumerate(
         (
-            (q_a_hbm, q_a), (k_a_hbm, k_a), (v_a_hbm, v_a),
-            (q_b_hbm, q_b), (k_b_hbm, k_b), (v_b_hbm, v_b),
+            (q_a_hbm, pack_a.at[:, 0]), (k_a_hbm, pack_a.at[:, 1]), (v_a_hbm, pack_a.at[:, 2]),
+            (q_b_hbm, pack_b.at[:, 0]), (k_b_hbm, pack_b.at[:, 1]), (v_b_hbm, pack_b.at[:, 2]),
             (ids_hbm, ids), (route_hbm, route), (cum_a_hbm, cum_a), (cum_b_hbm, cum_b),
             (wa_hbm, wa), (wb_hbm, wb), (residual_hbm, residual), (gain_hbm, gain),
             (gate_hbm.at[0], gw), (up_hbm.at[0], uw), (down_hbm.at[0], dw),
@@ -229,7 +222,7 @@
 
     for copy in loads[:6]:
         copy.wait()
-    sources = ((q_a, k_a, v_a), (q_b, k_b, v_b))
+    packs = (pack_a, pack_b)
     got = (got_a, got_b)
     sizes = (da, db)
 
@@ -238,13 +231,9 @@
         for k in range(1, n_sp):
             target = (s + k) % n_sp
             kind = (core + k) % 2
-            d = sizes[kind]
-            rows = pl.ds(pl.multiple_of((target // 2) * d, d), d)
-            for m in range(3):
-                copies.append(remote(
-                    sources[kind][m].at[rows], got[kind].at[m, s],
-                    qkv_send.at[m, k], qkv_recv.at[m, s], target, t,
-                ))
+            copies.append(remote(
+                packs[kind].at[target // 2], got[kind].at[s], qkv_send.at[k], qkv_recv.at[s], target, t
+            ))
         return copies
 
     for core in range(2):
@@ -252,10 +241,7 @@
         def _(core=core):
             for copy in qkv_copies(core):
                 copy.start()
-            d = sizes[core]
-            rows = pl.ds(pl.multiple_of(z * d, d), d)
-            for m in range(3):
-                got[core][m, s] = sources[core][m][rows, :]
+            got[core][s] = packs[core][z]
 
     loads[6].wait()
     loads[7].wait()
@@ -329,15 +315,13 @@
             for src in (2 * step, 2 * step + 1):
                 @pl.when(s != src)
                 def _(src=src):
-                    for m in range(3):
-                        remote(
-                            ref.at[m, src], ref.at[m, src],
-                            qkv_send.at[m, 0], qkv_recv.at[m, src], src, t,
-                        ).wait_recv()
+                    remote(
+                        ref.at[src], ref.at[src], qkv_send.at[0], qkv_recv.at[src], src, t
+                    ).wait_recv()
             for src in (2 * step, 2 * step + 1):
-                keys_t.append(jnp.transpose(ref[1, src]))
-                values.append(ref[2, src])
-            queries = jnp.concatenate([ref[0, 2 * step], ref[0, 2 * step + 1]], axis=1)
+                keys_t.append(jnp.transpose(ref[src, 1]))
+                values.append(ref[src, 2])
+            queries = jnp.concatenate([ref[2 * step, 0], ref[2 * step + 1, 0]], axis=1)
             count = span * (step + 1)
             keys = jnp.concatenate(keys_t, axis=0)
             vals = jnp.concatenate(values, axis=1)
@@ -438,34 +422,53 @@
         d_copies.append(copy)
     xs[c, t, z] = dsend[z]
     mate = 2 * z + 1 - c
-    ag_copies = []
-    pair_copies = []
-    for k in range(nz):
-        zs = (z + nz - k) % nz
+    near = [t, tp_to(1), tp_to(2), tp_to(3)]
+    half = slots // 2
+    ag_copies = [[] for _ in range(nz)]
+    pair_copies = [[] for _ in range(nz)]
+    h_copies = [[] for _ in range(nz)]
+    e_copies = []
+    r_copies = []
+
+    def source_chip(k):
+        return (z + nz - k) % nz
+
+    def to_pair(k, j):
+        block = xs.at[c, near[j], source_chip(k)]
+        copy = remote(block, block, pair_send.at[j, k], pair_recv.at[j, k], mate, t)
+        copy.start()
+        pair_copies[k].append(copy)
+
+    def to_near(ref, j, sends, recvs, k, i, copies):
+        copy = remote(ref, ref, sends.at[i, k], recvs.at[i, k], s, near[j])
+        copy.start()
+        copies[k].append(copy)
+
+    def tokens_out(k):
         if k:
             d_copies[k - 1].wait_recv()
-        block = xs.at[c, t, zs]
-        row = []
-        for j in range(1, n_tp):
-            copy = remote(block, block, ag_send.at[j - 1, k], ag_recv.at[j - 1, k], s, tp_to(j))
-            copy.start()
-            row.append(copy)
-        ag_copies.append(row)
-        copy = remote(block, block, pair_send.at[0, k], pair_recv.at[0, k], mate, t)
-        copy.start()
-        pair_copies.append([copy])
-
-    loads[14].wait()
-    loads[15].wait()
-    h_copies = []
-    for k in range(nz):
-        zs = (z + nz - k) % nz
-        for j in range(1, n_tp):
-            ag_copies[k][j - 1].wait_recv()
-            block = xs.at[c, tp_from(j), zs]
-            copy = remote(block, block, pair_send.at[j, k], pair_recv.at[j, k], mate, t)
-            copy.start()
-            pair_copies[k].append(copy)
+        block = xs.at[c, t, source_chip(k)]
+        to_near(block, 1, ag_send, ag_recv, k, 0, ag_copies)
+        to_near(block, 2, ag_send, ag_recv, k, 1, ag_copies)
+        to_pair(k, 0)
+
+    def tokens_relay(k):
+        zs = source_chip(k)
+        ag_copies[k][0].wait_recv()
+        to_near(xs.at[c, near[1], zs, pl.ds(0, half)], 2, ag_send, ag_recv, k, 2, ag_copies)
+        to_pair(k, 1)
+        ag_copies[k][1].wait_recv()
+        to_near(xs.at[c, near[2], zs, pl.ds(half, half)], 1, ag_send, ag_recv, k, 3, ag_copies)
+        to_pair(k, 2)
+
+    def hidden_out(k):
+        zs = source_chip(k)
+        ag_copies[k][2].wait_recv()
+        ag_copies[k][3].wait_recv()
+        to_pair(k, 3)
+        if k == 0:
+            loads[14].wait()
+            loads[15].wait()
         for j in range(n_tp):
             pair_copies[k][j].wait_recv()
         rows = [
@@ -476,19 +479,22 @@
         upper = jnp.dot(rows, uw[...], preferred_element_type=F32)
         hid[zs, t] = (gate / (1.0 + jnp.exp(-gate)) * upper).astype(BF16)
         block = hid.at[zs, t]
-        row = []
-        for j in range(1, n_tp):
-            copy = remote(block, block, h_send.at[j - 1, k], h_recv.at[j - 1, k], s, tp_to(j))
-            copy.start()
-            row.append(copy)
-        h_copies.append(row)
-
-    loads[16].wait()
-    e_copies = []
-    for k in range(nz):
-        zs = (z + nz - k) % nz
-        for copy in h_copies[k]:
-            copy.wait_recv()
+        to_near(block, 1, h_send, h_recv, k, 0, h_copies)
+        to_near(block, 2, h_send, h_recv, k, 1, h_copies)
+
+    def hidden_relay(k):
+        zs = source_chip(k)
+        h_copies[k][0].wait_recv()
+        to_near(hid.at[zs, near[1], pl.ds(0, slots)], 2, h_send, h_recv, k, 2, h_copies)
+        h_copies[k][1].wait_recv()
+        to_near(hid.at[zs, near[2], pl.ds(slots, slots)], 1, h_send, h_recv, k, 3, h_copies)
+
+    def down(k):
+        zs = source_chip(k)
+        h_copies[k][2].wait_recv()
+        h_copies[k][3].wait_recv()
+        if k == 0:
+            loads[16].wait()
         rows = jnp.concatenate([hid[zs, i] for i in range(n_tp)], axis=1)
         result = jnp.dot(rows, dw[...], preferred_element_type=F32)
         top = result[:slots]
@@ -499,9 +505,8 @@
         copy.start()
         e_copies.append(copy)
 
-    r_copies = []
-    for k in range(nz):
-        zs = (z + nz - k) % nz
+    def give_back(k):
+        zs = source_chip(k)
         if k:
             w_copies[k - 1].wait_recv()
         e_copies[k].wait_recv()
@@ -511,16 +516,24 @@
         own_w = jnp.where(c == 0, w0, w1)
         mate_w = jnp.where(c == 0, w1, w0)
         total = (own_w * own[zs] + mate_w * part_got[zs].astype(F32)).astype(BF16)
+        here_rows = pl.ds(pl.multiple_of(z * slots, slots), slots)
         if k:
             ret_send[k] = total
             copy = remote(
-                ret_send.at[k], ret.at[pl.ds(pl.multiple_of(z * slots, slots), slots)],
-                r_send.at[k], r_recv.at[k], 2 * zs + c, t,
+                ret_send.at[k], ret.at[here_rows], r_send.at[k], r_recv.at[k], 2 * zs + c, t
             )
             copy.start()
             r_copies.append(copy)
         else:
-            ret[pl.ds(pl.multiple_of(z * slots, slots), slots), :] = total
+            ret[here_rows, :] = total
+
+    for i in range(nz + 3):
+        for stage, lag in (
+            (tokens_out, 0), (tokens_relay, 1), (hidden_relay, 2), (hidden_out, 1), (down, 2),
+            (give_back, 3),
+        ):
+            if 0 <= i - lag < nz:
+                stage(i - lag)
 
     for k in range(1, nz):
         r_copies[k - 1].wait_recv()
@@ -561,18 +574,17 @@
     slots = tok // TOP
     pieces = 2
     width = model // pieces
-    dims = (n_sp, n_tp, cumlog_a.shape[0], HDA, HDB, group_size)
+    heads = cumlog_a.shape[0]
+    grid_a = (heads, HDA, tok)
+    grid_b = (heads, HDB, tok)
+    dims = (n_sp, n_tp, heads, HDA, HDB, group_size)
     vmem = pl.BlockSpec(memory_space=pltpu.VMEM)
     anyw = pl.BlockSpec(memory_space=pl.ANY)
     dma = pltpu.SemaphoreType.DMA
     scratch = [
-        pltpu.VMEM(query_a.shape, BF16),
-        pltpu.VMEM(key_a.shape, BF16),
-        pltpu.VMEM(value_a.shape, BF16),
+        pltpu.VMEM((heads, 3, HDA, tok), BF16),
         pltpu.VMEM(cumlog_a.shape, F32),
-        pltpu.VMEM(query_b.shape, BF16),
-        pltpu.VMEM(key_b.shape, BF16),
-        pltpu.VMEM(value_b.shape, BF16),
+        pltpu.VMEM((heads, 3, HDB, tok), BF16),
         pltpu.VMEM(cumlog_b.shape, F32),
         pltpu.VMEM(residual.shape, BF16),
         pltpu.VMEM((1, model), F32),
@@ -583,8 +595,8 @@
         pltpu.VMEM(gate_w.shape[1:], BF16),
         pltpu.VMEM(up_w.shape[1:], BF16),
         pltpu.VMEM(down_w.shape[1:], BF16),
-        pltpu.VMEM((3, n_sp, HDA, tok), BF16),
-        pltpu.VMEM((3, n_sp, HDB, tok), BF16),
+        pltpu.VMEM((n_sp, 3, HDA, tok), BF16),
+        pltpu.VMEM((n_sp, 3, HDB, tok), BF16),
         pltpu.VMEM((n_sp * tok, tok), F32),
         pltpu.VMEM((n_sp, HDA, tok), BF16),
         pltpu.VMEM((n_sp, HDB, tok), BF16),
@@ -606,15 +618,15 @@
         pltpu.VMEM((nz, slots, feat), BF16),
         pltpu.VMEM((nz * slots, feat), BF16),
         dma((17,)),
-        dma((3, n_sp)), dma((3, n_sp)),
+        dma((n_sp,)), dma((n_sp,)),
         dma((n_sp,)), dma((n_sp,)),
         dma((pieces, n_tp - 1)), dma((pieces, n_tp - 1)),
         dma((n_tp - 1,)), dma((n_tp - 1,)),
         dma((nz,)), dma((nz,)),
         dma((nz,)), dma((nz,)),
-        dma((n_tp - 1, nz)), dma((n_tp - 1, nz)),
+        dma((4, nz)), dma((4, nz)),
         dma((n_tp, nz)), dma((n_tp, nz)),
-        dma((n_tp - 1, nz)), dma((n_tp - 1, nz)),
+        dma((4, nz)), dma((4, nz)),
         dma((nz,)), dma((nz,)),
         dma((nz,)), dma((nz,)),
     ]
@@ -628,7 +640,8 @@
             collective_id=0, has_side_effects=True, vmem_limit_bytes=67043328
         ),
     )(
-        query_a, key_a, value_a, cumlog_a, query_b, key_b, value_b, cumlog_b, residual,
+        query_a.reshape(grid_a), key_a.reshape(grid_a), value_a.reshape(grid_a), cumlog_a,
+        query_b.reshape(grid_b), key_b.reshape(grid_b), value_b.reshape(grid_b), cumlog_b, residual,
         norm_gain.reshape(1, -1), expert_ids.T, route_weight.T, out_weight_a, out_weight_b,
         gate_w, up_w, down_w,
     )
@@ -639,7 +652,7 @@
     heads_a = args[3].shape[0]
     heads_b = args[7].shape[0]
     fits = heads_a == heads_b and heads_a + heads_b == n_sp
-    fits = fits and n_sp == GROUPS * TOP and n_sp == 2 * GROUPS
+    fits = fits and lax.axis_size("tp") == 4 and n_sp == GROUPS * TOP and n_sp == 2 * GROUPS
     return (fused if fits else per_device)(*args)
 
 

time: 77.4 us -> 85.4 us (1.10)
  Pallas kernels: 75.7 us -> 83.7 us
    pallas_call x1, Pallas kernels: 75.7 us -> 83.7 us  [fused(): pl.pallas_call(functools.partial(fused_kernel, dims), out_shape=jax.Shape...]
where the time goes in v3:
time: 85.4 us; the launch traced here: 85.3 us
  Pallas kernels  83.7 us (98%)
  local copies, waits for them, and re-layouts  1.57 us (2%)
    pallas_call x1, Pallas kernels, fused(): pl.pallas_call(functools.partial(fused_kernel, dims), out_shape=jax.Shape...  83.7 us

profile of v3, /device:TPU:0, one launch (start us, length us, event | category | flops | bytes accessed | tf_op | source)
XLA Modules:
  0.0 85.3 jit_solution(13110441073886220057)
XLA Ops:
  0.0 83.7 %shard_map.163 = bf16[128,512]{1,0:T(8,128)(2,1)} custom-call(bf16[4,64,128]{2,1,0:T(8,128)(2,1)} %bitcast.12, bf16[4,64,128]{2,1,0:T(8,128)(2,1)} %bitcast.13, bf16[4,64,128]{2,1,0:T(8,128)(2,1)} %bitcast.14, f32[4,1024]{1,0:T(4,128)} %cum_a_hbm.1, bf16[4,128,128]{2,1,0:T(8,128)(2,1)} %bitcast.9, bf16[4,128,128]{2,1,0:T(8,128)(2,1)} %bitcast.10, ...), custom_call_target="tpu_custom_call" | custom-call | tf_op jit(solution)/shard_map/pallas_call | solution.py:633
  83.7 1.6 %copy.19 = bf16[128,512]{1,0:T(8,128)(2,1)} copy(bf16[128,512]{1,0:T(8,128)(2,1)} %shard_map.163) | data formatting | bytes 262144

commit v4 on v3

--- a/solution.py
+++ b/solution.py
@@ -423,7 +423,6 @@
     xs[c, t, z] = dsend[z]
     mate = 2 * z + 1 - c
     near = [t, tp_to(1), tp_to(2), tp_to(3)]
-    half = slots // 2
     ag_copies = [[] for _ in range(nz)]
     pair_copies = [[] for _ in range(nz)]
     h_copies = [[] for _ in range(nz)]
@@ -448,24 +447,15 @@
         if k:
             d_copies[k - 1].wait_recv()
         block = xs.at[c, t, source_chip(k)]
-        to_near(block, 1, ag_send, ag_recv, k, 0, ag_copies)
-        to_near(block, 2, ag_send, ag_recv, k, 1, ag_copies)
+        for j in range(1, n_tp):
+            to_near(block, j, ag_send, ag_recv, k, j - 1, ag_copies)
         to_pair(k, 0)
-
-    def tokens_relay(k):
-        zs = source_chip(k)
-        ag_copies[k][0].wait_recv()
-        to_near(xs.at[c, near[1], zs, pl.ds(0, half)], 2, ag_send, ag_recv, k, 2, ag_copies)
-        to_pair(k, 1)
-        ag_copies[k][1].wait_recv()
-        to_near(xs.at[c, near[2], zs, pl.ds(half, half)], 1, ag_send, ag_recv, k, 3, ag_copies)
-        to_pair(k, 2)
 
     def hidden_out(k):
         zs = source_chip(k)
-        ag_copies[k][2].wait_recv()
-        ag_copies[k][3].wait_recv()
-        to_pair(k, 3)
+        for j in range(1, n_tp):
+            ag_copies[k][j - 1].wait_recv()
+            to_pair(k, j)
         if k == 0:
             loads[14].wait()
             loads[15].wait()
@@ -479,20 +469,13 @@
         upper = jnp.dot(rows, uw[...], preferred_element_type=F32)
         hid[zs, t] = (gate / (1.0 + jnp.exp(-gate)) * upper).astype(BF16)
         block = hid.at[zs, t]
-        to_near(block, 1, h_send, h_recv, k, 0, h_copies)
-        to_near(block, 2, h_send, h_recv, k, 1, h_copies)
-
-    def hidden_relay(k):
-        zs = source_chip(k)
-        h_copies[k][0].wait_recv()
-        to_near(hid.at[zs, near[1], pl.ds(0, slots)], 2, h_send, h_recv, k, 2, h_copies)
-        h_copies[k][1].wait_recv()
-        to_near(hid.at[zs, near[2], pl.ds(slots, slots)], 1, h_send, h_recv, k, 3, h_copies)
+        for j in range(1, n_tp):
+            to_near(block, j, h_send, h_recv, k, j - 1, h_copies)
 
     def down(k):
         zs = source_chip(k)
-        h_copies[k][2].wait_recv()
-        h_copies[k][3].wait_recv()
+        for copy in h_copies[k]:
+            copy.wait_recv()
         if k == 0:
             loads[16].wait()
         rows = jnp.concatenate([hid[zs, i] for i in range(n_tp)], axis=1)
@@ -527,13 +510,15 @@
         else:
             ret[here_rows, :] = total
 
-    for i in range(nz + 3):
-        for stage, lag in (
-            (tokens_out, 0), (tokens_relay, 1), (hidden_relay, 2), (hidden_out, 1), (down, 2),
-            (give_back, 3),
-        ):
-            if 0 <= i - lag < nz:
-                stage(i - lag)
+    for k in range(nz):
+        tokens_out(k)
+    for k in range(nz):
+        hidden_out(k)
+    for i in range(nz + 1):
+        if i < nz:
+            down(i)
+        if i:
+            give_back(i - 1)
 
     for k in range(1, nz):
         r_copies[k - 1].wait_recv()

time: 85.4 us -> 76.4 us (0.89)
  Pallas kernels: 83.7 us -> 74.6 us
    pallas_call x1, Pallas kernels: 83.7 us -> 74.6 us  [fused(): pl.pallas_call(functools.partial(fused_kernel, dims), out_shape=jax.Shape...]
where the time goes in v4:
time: 76.4 us; the launch traced here: 76.2 us
  Pallas kernels  74.6 us (98%)
  local copies, waits for them, and re-layouts  1.57 us (2%)
    pallas_call x1, Pallas kernels, fused(): pl.pallas_call(functools.partial(fused_kernel, dims), out_shape=jax.Shape...  74.6 us
    unnamed x1, local copies, waits for them, and re-layouts  1.57 us

profile of v4, /device:TPU:0, one launch (start us, length us, event | category | flops | bytes accessed | tf_op | source)
XLA Modules:
  0.0 76.2 jit_solution(5985523936415823560)
XLA Ops:
  0.0 74.6 %shard_map.163 = bf16[128,512]{1,0:T(8,128)(2,1)} custom-call(bf16[4,64,128]{2,1,0:T(8,128)(2,1)} %bitcast.12, bf16[4,64,128]{2,1,0:T(8,128)(2,1)} %bitcast.13, bf16[4,64,128]{2,1,0:T(8,128)(2,1)} %bitcast.14, f32[4,1024]{1,0:T(4,128)} %cum_a_hbm.1, bf16[4,128,128]{2,1,0:T(8,128)(2,1)} %bitcast.9, bf16[4,128,128]{2,1,0:T(8,128)(2,1)} %bitcast.10, ...), custom_call_target="tpu_custom_call" | custom-call | tf_op jit(solution)/shard_map/pallas_call | solution.py:618
  74.7 1.6 %copy.19 = bf16[128,512]{1,0:T(8,128)(2,1)} copy(bf16[128,512]{1,0:T(8,128)(2,1)} %shard_map.163) | data formatting | bytes 262144
